TPU v7x, 256 devices: a 4x2x16 block of a 4x16x16 slice. The times are simulated.
256 devices in a mesh: grp: 2 (over y), sp: 32 (over z, core), tp: 4 (over x).
Axes of the slice: x: 4, y: 2, z: 16, core: 2. Of those that a mesh axis runs over, the one named last changes fastest.
The devices are a block of a 4x16x16 slice.
Arguments:
- residual_in: bfloat16 [8192, 2048], P(('grp', 'sp'), 'tp'), parts along dimension 0, may hold values from -16 to 16
- query_pre: bfloat16 [8192, 512], P(('grp', 'sp'), 'tp'), parts along dimension 0, may hold values from -6 to 6
- forget_pre: bfloat16 [8192, 512], P(('grp', 'sp'), 'tp'), parts along dimension 0, may hold values from -9 to 9
- value_pre: bfloat16 [8192, 512], P(('grp', 'sp'), 'tp'), parts along dimension 0, may hold values from -6 to 6
- gate_pre: bfloat16 [8192, 512], P(('grp', 'sp'), 'tp'), parts along dimension 0, may hold values from -6 to 6
- floor_gap: float32 [512], P('tp'), may hold values from 0 to 1, as said below
- head_gain: float32 [64], replicated, may hold values from 0.1 to 1.9
- out_weight: bfloat16 [512, 2048], P(None, 'tp'), may hold values from -0.25 to 0.25
- norm_gain: float32 [2048], P('tp'), may hold values from 0.1 to 1.9
- value_weight: bfloat16 [2048, 5632], P('sp', 'tp'), may hold values from -0.125 to 0.125
- gate_weight: bfloat16 [2048, 5632], P('sp', 'tp'), may hold values from -0.125 to 0.125
- value_taps: float32 [3, 5632], P(None, 'tp'), may hold values from -3 to 3
- gate_taps: float32 [3, 5632], P(None, 'tp'), may hold values from -3 to 3
- down_weight: bfloat16 [5632, 2048], P('tp', 'sp'), may hold values from -0.078125 to 0.078125
Outputs:
- mixed: bfloat16 [8192, 2048], P(('grp', 'sp'), 'tp'), parts along dimension 0
There are 2 independent parts, one for each index of `grp`. A program takes and returns all parts, laid end to end along the dimension named above; an argument that names none is the same for every part. Nothing has to cross between parts.
Inputs may be any that keep to these rules, and one draw needn't show every extreme that they name: `floor_gap`: each channel's value lies strictly between 0 and 1.
All inputs are finite; a program needn't handle non-finite values.
Results may differ from a plain program's by a relative error of at most 0.0085.
Values may be sent and summed in bfloat16 or wider, within the bound.
No kernel may reach another device: no remote copies, remote signals or barrier semaphores. Data moves between devices by JAX's collectives and lax.ppermute only.
A program may use at most 128 MiB of HBM per device.

v0:
```python
import jax
import jax.numpy as jnp
from jax import lax
from jax.sharding import Mesh
from jax.sharding import PartitionSpec as P

D = 2048
DK = 64
DV = 64
BLOCK = 64
SP = ("sp_0", "sp_1")
GRP_SP = ("grp", "sp_0", "sp_1")


epsilon = 1e-06
highest_precision = lax.Precision.HIGHEST


def nothing_yet(array, identity):
    return jax.tree.map(
        lambda a, e: jnp.broadcast_to(jnp.asarray(e, a.dtype), a.shape), array, identity
    )


def all_in_one(array, axis):
    leaves = jax.tree.leaves(array)
    sequence = sorted(range(len(leaves)), key=lambda k: -leaves[k].size)
    width = (1, *leaves[sequence[0]].shape)[-1]
    lines = [
        jnp.pad(leaves[k].reshape(-1), (0, -leaves[k].size % width)).reshape(-1, width)
        for k in sequence
    ]
    both, at, found = (lax.all_gather(jnp.concatenate(lines), axis), 0, {})
    for k, line in zip(sequence, lines):
        share = both[:, at : at + len(line)].reshape(len(both), -1)
        found[k] = share[:, : leaves[k].size].reshape(-1, *leaves[k].shape)
        at += len(line)
    numbers = iter(range(len(leaves)))
    return jax.tree.map(lambda _: found[next(numbers)], array)


def entering(array, axes, combine, identity):
    before = start = nothing_yet(array, identity)
    so_far = array
    for axis in reversed(axes):
        length, place = (lax.axis_size(axis), lax.axis_index(axis))
        pieces = all_in_one(so_far, axis)
        inside, so_far = (start, start)
        for k in range(length):
            passed = k < place
            so_far = combine(so_far, jax.tree.map(lambda part: part[k], pieces))
            inside = jax.tree.map(lambda new, old: jnp.where(passed, new, old), so_far, inside)
        before = combine(inside, before)
    return before


def joined_along(pieces, dim):
    pieces = jnp.moveaxis(pieces, 0, dim)
    dims = pieces.shape
    return pieces.reshape(*dims[:dim], dims[dim] * dims[dim + 1], *dims[dim + 2 :])


def copy_for_each(array, axis):
    copies = jnp.broadcast_to(array, (lax.axis_size(axis), *array.shape))
    return lax.all_to_all(copies, axis, split_axis=0, concat_axis=0, tiled=True)


def collect(array, axis, dim):
    return joined_along(copy_for_each(array, axis), dim)


def taken_together(array, axis):
    return copy_for_each(array, axis).sum(axis=0)


def in_one_piece(arrays, axis, dim, along):
    widths = [a.shape[along] for a in arrays]
    both = jnp.concatenate(arrays, axis=along)
    out = lax.all_gather(both, axis, axis=dim, tiled=True)
    return tuple(jnp.split(out, [sum(widths[:k]) for k in range(1, len(widths))], axis=along))


def shifted(array, axis, by):
    length = lax.axis_size(axis)
    pairs = [(i, i + by) for i in range(length) if 0 <= i + by < length]
    return lax.ppermute(array, axis, pairs)


def split_up(array, dim, length):
    dims = array.shape
    pieces = array.reshape(*dims[:dim], length, dims[dim] // length, *dims[dim + 1 :])
    return jnp.moveaxis(pieces, dim, 0)


def summed_on_arrival(array, axis, dim):
    length = lax.axis_size(axis)
    pieces = lax.all_to_all(split_up(array, dim, length), axis, 0, 0, tiled=True)
    return jnp.sum(pieces.astype(jnp.float32), axis=0)


def split_heads(matrix, head_count):
    return matrix.reshape(matrix.shape[0], head_count, -1).transpose(1, 0, 2)


def recurrence(query_rows, gate_keys, values, log_decay, block_size, start_state):
    head_count, seq_length, key_width = query_rows.shape
    block_count = seq_length // block_size

    def to_blocks(tensor):
        return tensor.reshape(head_count, block_count, block_size, tensor.shape[-1]).transpose(
            1, 0, 2, 3
        )

    causal = jnp.tril(jnp.ones((block_size, block_size), dtype=bool))

    def advance(current_state, inputs):
        block_queries, block_keys, block_values, decay_block = inputs
        running_state = jnp.cumsum(decay_block, axis=1)
        carried_state = jnp.einsum(
            "pen,pnd->ped",
            block_queries * jnp.exp(running_state),
            current_state,
            precision=highest_precision,
        )
        spread = jnp.where(
            causal[None, :, :, None],
            running_state[:, :, None, :] - running_state[:, None, :, :],
            -jnp.inf,
        )
        scores = jnp.einsum(
            "htk,hsk,htsk->hts",
            block_queries,
            block_keys,
            jnp.exp(spread),
            precision=highest_precision,
        )
        inner = jnp.einsum("hts,hsv->htv", scores, block_values, precision=highest_precision)
        ending_state = running_state[:, -1, :]
        fresh_update = jnp.einsum(
            "bia,big->bag",
            block_keys * jnp.exp(ending_state[:, None, :] - running_state),
            block_values,
            precision=highest_precision,
        )
        return (
            jnp.exp(ending_state)[:, :, None] * current_state + fresh_update,
            carried_state + inner,
        )

    final_state, outputs = lax.scan(
        advance,
        start_state,
        (to_blocks(query_rows), to_blocks(gate_keys), to_blocks(values), to_blocks(log_decay)),
    )
    return (
        final_state,
        outputs.transpose(1, 0, 2, 3).reshape(head_count, seq_length, values.shape[-1]),
    )


def mixer_inputs(query_pre, forget_pre, value_pre, floor_gap, head_count):
    gate_keys = floor_gap * jax.nn.sigmoid(-forget_pre.astype(jnp.float32))
    log_decay = jnp.log1p(-gate_keys)
    query_rows = jax.nn.silu(query_pre.astype(jnp.float32))
    return (
        split_heads(query_rows, head_count),
        split_heads(gate_keys, head_count),
        split_heads(value_pre.astype(jnp.float32), head_count),
        split_heads(log_decay, head_count),
    )


def head_output(recurrent, head_gain, gate_pre):
    ordered = recurrent.transpose(1, 0, 2)
    scaled = (
        ordered
        * lax.rsqrt(jnp.mean(ordered * ordered, axis=-1, keepdims=True) + epsilon)
        * head_gain
    )
    gating = jax.nn.silu(gate_pre.astype(jnp.float32)).reshape(ordered.shape)
    return (scaled * gating).reshape(ordered.shape[0], -1).astype(jnp.bfloat16)


def causal_taps(padded, taps, row_count):
    return (
        taps[0] * padded[0:row_count]
        + taps[1] * padded[1 : row_count + 1]
        + taps[2] * padded[2 : row_count + 2]
    )


def join_states(earlier, later):
    return (earlier[0] * later[0], later[0][:, :, None] * earlier[1] + later[1])


def on_device(
    residual_in,
    query_pre,
    forget_pre,
    value_pre,
    gate_pre,
    floor_gap,
    head_gain,
    out_weight,
    norm_gain,
    value_weight,
    gate_weight,
    value_taps,
    gate_taps,
    down_weight,
):
    row_count = residual_in.shape[0]
    local_heads = floor_gap.shape[0] // DK
    query_rows, gate_keys, values, log_decay = mixer_inputs(
        query_pre, forget_pre, value_pre, floor_gap, local_heads
    )
    zero_state = jnp.zeros((local_heads, DK, DV), jnp.float32)
    final_state, recurrent = recurrence(query_rows, gate_keys, values, log_decay, BLOCK, zero_state)
    decay_from_start = jnp.cumsum(log_decay, axis=1)
    total_decay = jnp.exp(decay_from_start[:, -1, :])
    entering_state = entering(
        (total_decay, final_state), SP, join_states, (jnp.ones_like(total_decay), zero_state)
    )[1]
    recurrent = recurrent + jnp.einsum(
        "pen,pnd->ped",
        query_rows * jnp.exp(decay_from_start),
        entering_state,
        precision=highest_precision,
    )
    head_out = head_output(recurrent, head_gain, gate_pre)
    projected = jnp.dot(collect(head_out, "tp", 1), out_weight, preferred_element_type=jnp.float32)
    stream = residual_in.astype(jnp.float32) + projected
    squares = taken_together(jnp.sum(stream * stream, axis=1), "tp")
    normed_part = (stream * lax.rsqrt(squares / D + epsilon)[:, None] * norm_gain).astype(
        jnp.bfloat16
    )
    normed = collect(normed_part, "tp", 1)
    pieces = in_one_piece((value_weight, gate_weight), SP, 0, 1)
    sum_value = jnp.dot(normed, pieces[0], preferred_element_type=jnp.float32)
    sum_gate = jnp.dot(normed, pieces[1], preferred_element_type=jnp.float32)
    up_value = sum_value.astype(jnp.bfloat16)
    up_gate = sum_gate.astype(jnp.bfloat16)
    hidden_width = up_value.shape[1]
    tail_rows = jnp.concatenate([up_value[row_count - 2 :], up_gate[row_count - 2 :]], axis=1)
    before = shifted(tail_rows, SP, 1)
    padded_value = jnp.concatenate([before[:, :hidden_width], up_value], axis=0).astype(jnp.float32)
    padded_gate = jnp.concatenate([before[:, hidden_width:], up_gate], axis=0).astype(jnp.float32)
    conv_value = causal_taps(padded_value, value_taps, row_count)
    conv_gate = causal_taps(padded_gate, gate_taps, row_count)
    hidden = (jax.nn.silu(conv_gate) * conv_value).astype(jnp.bfloat16)
    terms = jnp.dot(
        hidden,
        lax.all_gather(down_weight, SP, axis=1, tiled=True),
        preferred_element_type=jnp.float32,
    )
    down_part = summed_on_arrival(terms.astype(jnp.bfloat16), "tp", 1)
    return (stream + down_part).astype(jnp.bfloat16)


def solution(mesh):
    finer = Mesh(
        mesh.devices.reshape(mesh.shape["grp"], 16, 2, mesh.shape["tp"]),
        ("grp", "sp_0", "sp_1", "tp"),
    )
    placed = (
        P(GRP_SP, "tp"),
        P(GRP_SP, "tp"),
        P(GRP_SP, "tp"),
        P(GRP_SP, "tp"),
        P(GRP_SP, "tp"),
        P("tp"),
        P(),
        P(None, "tp"),
        P("tp"),
        P(SP, "tp"),
        P(SP, "tp"),
        P(None, "tp"),
        P(None, "tp"),
        P("tp", SP),
    )
    return jax.shard_map(
        on_device, mesh=finer, in_specs=placed, out_specs=P(GRP_SP, "tp"), check_vma=False
    )
```

profile of v0, /device:TPU:38, one launch (start us, length us, event | category | flops | bytes accessed | tf_op | source)
XLA Modules:
  0.0 211.2 jit_solution(9116344406348762954)
XLA Ops:
  6.6 1.9 pad_maximum_fusion
  8.6 0.7 all-gather.9.cloned.1.call-update
  9.3 0.9 copy.254
  10.2 0.8 divide_multiply_fusion
  11.0 0.1 reshape.163
  11.2 0.9 copy.256
  12.2 0.1 reshape.165
  12.4 0.9 copy.255
  13.3 0.1 reshape.176
  13.4 25.8 %while.13 = (s32[]{:T(128)}, f32[2,64,64]{2,1,0:T(8,128)S(1)}, f32[2,2,64,64]{3,2,1,0:T(8,128)S(1)}, f32[2,2,64,64]{2,0,3,1:T(2,128)S(1)}, f32[2,2,64,64]{2,0,3,...) while((s32[]{:T(128)}, f32[2,64,64]{2,1,0:T(8,128)S(1)}, ...), condition=%wide.region_2.3_spmd.clone, body=%wide.region_0.2_spmd.clone.sunk | while | flops 22073348 | bytes 9710728 | solution.py:150
  13.6 0.1 reduce_window_sum.25
  13.7 2.9 %select_exponential_fusion.2 = f32[2,64,64,64]{3,2,1,0:T(8,128)} fusion(f32[2,64,64]{2,1,0:T(8,128)S(1)} %reduce_window_sum.25, pred[64,64]{1,0:T(8,128)(4,1)S(1)} %iota_compare_fusion.2), kind=kLoop, calls=%fused_computation.3.clone.1 | loop fusion | flops 1048576 | bytes 2134016 | tf_op jit(solution)/shard_map/while/body/eval_jaxpr/exp | solution.py:134
  16.6 5.6 %copy.451 = f32[2,64,64,64]{1,2,3,0:T(8,128)} copy(f32[2,64,64,64]{3,2,1,0:T(8,128)} %select_exponential_fusion.2) | data formatting | bytes 4194304 | tf_op jit(solution)/shard_map/while
  22.2 0.1 constant_dynamic-slice_fusion.5
  22.5 2.9 %fusion.153 = f32[2,64,64]{1,2,0:T(8,128)S(1)} fusion(f32[2,64,64,64]{1,2,3,0:T(8,128)} %copy.451, f32[2,64,64]{2,1,0:T(8,128)S(1)} %copy.452, f32[2,64,64]{2,1,0:T(8,128)S(1)} %bitcast.190), kind=kLoop, calls=%fused_computation.2.clone.1 | loop fusion | flops 1564672 | bytes 2195456 | tf_op jit(solution)/shard_map/while/body/eval_jaxpr/htk,hsk,htsk->hts/dot_general | solution.py:130
  25.4 0.2 fusion.152
  25.6 0.3 fusion.154
  26.0 0.3 convolution_add_fusion.5
  26.5 0.1 reduce_window_sum.25
  26.6 2.9 %select_exponential_fusion.2 = f32[2,64,64,64]{3,2,1,0:T(8,128)} fusion(f32[2,64,64]{2,1,0:T(8,128)S(1)} %reduce_window_sum.25, pred[64,64]{1,0:T(8,128)(4,1)S(1)} %iota_compare_fusion.2), kind=kLoop, calls=%fused_computation.3.clone.1 | loop fusion | flops 1048576 | bytes 2134016 | tf_op jit(solution)/shard_map/while/body/eval_jaxpr/exp | solution.py:134
  29.5 5.6 %copy.451 = f32[2,64,64,64]{1,2,3,0:T(8,128)} copy(f32[2,64,64,64]{3,2,1,0:T(8,128)} %select_exponential_fusion.2) | data formatting | bytes 4194304 | tf_op jit(solution)/shard_map/while
  35.2 0.1 constant_dynamic-slice_fusion.5
  35.4 2.9 %fusion.153 = f32[2,64,64]{1,2,0:T(8,128)S(1)} fusion(f32[2,64,64,64]{1,2,3,0:T(8,128)} %copy.451, f32[2,64,64]{2,1,0:T(8,128)S(1)} %copy.452, f32[2,64,64]{2,1,0:T(8,128)S(1)} %bitcast.190), kind=kLoop, calls=%fused_computation.2.clone.1 | loop fusion | flops 1564672 | bytes 2195456 | tf_op jit(solution)/shard_map/while/body/eval_jaxpr/htk,hsk,htsk->hts/dot_general | solution.py:130
  38.3 0.2 fusion.152
  38.5 0.3 fusion.154
  38.9 0.3 convolution_add_fusion.5
  39.3 0.2 reduce_window_sum.22
  39.5 0.1 copy.265
  39.6 2.0 all-gather.2
  41.9 0.1 copy.269
  42.1 65.7 %all-gather.3 = f32[16,130,64]{1,2,0:T(8,128)S(1)} all-gather(f32[1,130,64]{1,2,0:T(8,128)S(1)} %maximum_bitcast_fusion.1), channel_id=3, replica_groups=mesh['grp'=2,'sp_0'=16,'sp_1'=2,'tp'=4] {'sp_0'}, dimensions={0}, use_global_device_ids=true | all-gather | bytes 565760 | tf_op jit(solution)/shard_map/all_gather | solution.py:33
  107.8 0.1 squeeze.100
  108.0 0.1 squeeze.102
  108.1 0.1 squeeze.103
  108.2 0.1 squeeze.104
  108.4 0.1 squeeze.90
  108.5 0.1 squeeze.91
  108.6 0.1 squeeze.92
  108.7 0.1 squeeze.93
  108.9 0.1 squeeze.95
  109.0 0.1 squeeze.96
  109.1 0.1 squeeze.97
  109.2 0.1 squeeze.98
  110.8 0.1 squeeze.105
  110.9 0.1 squeeze.106
  111.0 1.0 copy.262
  112.0 0.1 reshape.170
  112.2 0.9 copy.305
  113.0 0.5 multiply_reduce_fusion.1
  113.6 0.7 multiply_convert_fusion.1
  114.4 8.2 %all_to_all.21 = bf16[4,128,128]{1,2,0:T(8,128)(2,1)S(1)} all-to-all(bf16[4,128,128]{1,2,0:T(8,128)(2,1)S(1)} %broadcast_in_dim.56), channel_id=1, replica_groups=mesh['grp'=2,'sp_0'=16,'sp_1'=2,'tp'=4] {'tp'}, dimensions={0} | all-to-all | bytes 262144 | tf_op jit(solution)/shard_map/all_to_all | solution.py:65
  122.6 1.2 multiply_reduce_fusion
  123.9 7.6 %all_to_all.22 = f32[4,1,128]{2,1,0:T(1,128)S(1)} all-to-all(f32[4,1,128]{2,1,0:T(1,128)S(1)} %broadcast_in_dim.57), channel_id=1, replica_groups=mesh['grp'=2,'sp_0'=16,'sp_1'=2,'tp'=4] {'tp'}, dimensions={0} | all-to-all | bytes 4096 | tf_op jit(solution)/shard_map/all_to_all | solution.py:65
  131.6 0.1 copy.307
  131.8 10.5 %all_to_all.23 = bf16[4,128,512]{1,2,0:T(8,128)(2,1)S(1)} all-to-all(bf16[4,128,512]{1,2,0:T(8,128)(2,1)S(1)} %broadcast_in_dim.58), channel_id=1, replica_groups=mesh['grp'=2,'sp_0'=16,'sp_1'=2,'tp'=4] {'tp'}, dimensions={0} | all-to-all | bytes 1048576 | tf_op jit(solution)/shard_map/all_to_all | solution.py:65
  142.4 3.7 %fusion.20 = bf16[128,1408]{1,0:T(8,128)(2,1)S(1)} fusion(bf16[128,2048]{0,1:T(8,128)(2,1)S(1)} %bitcast.204, bf16[2048,2816]{1,0:T(8,128)(2,1)} %all-gather.7.cloned.1.call-done), kind=kOutput, calls=%fused_computation.30 | convolution fusion | flops 738377728 | bytes 6651904 | tf_op jit(solution)/shard_map/dot_general | solution.py:239
  146.1 3.7 %fusion.23 = bf16[128,1408]{1,0:T(8,128)(2,1)S(1)} fusion(bf16[128,2048]{0,1:T(8,128)(2,1)S(1)} %bitcast.205, bf16[2048,2816]{1,0:T(8,128)(2,1)} %all-gather.7.cloned.1.call-done), kind=kOutput, calls=%fused_computation.31 | convolution fusion | flops 738377728 | bytes 6651904 | tf_op jit(solution)/shard_map/dot_general | solution.py:240
  149.8 1.3 collective-permute-start
  151.2 0.7 collective-permute-done
  151.9 0.2 maximum_convert_fusion
  152.1 34.5 %all-gather.9.cloned.1.call-done = bf16[1408,2048]{0,1:T(8,128)(2,1)} async-done(((bf16[1408,64]{0,1:T(8,128)(2,1)}), bf16[1408,2048]{0,1:T(8,128)(2,1)}) %all-gather.9.cloned.1.call-update) | async-done | bytes 5767184 | tf_op jit(solution)/shard_map/all_gather | solution.py:253
  186.6 4.7 %convolution_convert_fusion = bf16[128,2048]{1,0:T(8,128)(2,1)S(1)} fusion(bf16[1408,2048]{0,1:T(8,128)(2,1)} %all-gather.9.cloned.1.call-done, f32[130,1408]{1,0:T(8,128)S(1)} %get-tuple-element.181, f32[130,1408]{1,0:T(8,128)S(1)} %get-tuple-element.180, f32[1408]{0:T(1024)S(1)} %get-tuple-element.115, f32[1408]{0:T(1024)S(1)} %get-tuple-element.116, ...), kind=kOutput, calls=%fused_computation.32 | convolution fusion | flops 741343232 | bytes 10665984 | tf_op jit(solution)/shard_map/dot_general | solution.py:251
  191.4 12.2 %all_to_all.24 = bf16[4,128,512]{2,1,0:T(8,128)(2,1)S(1)} all-to-all(bf16[4,128,512]{2,1,0:T(8,128)(2,1)S(1)} %bitcast.196), channel_id=1, replica_groups=mesh['grp'=2,'sp_0'=16,'sp_1'=2,'tp'=4] {'tp'}, dimensions={0} | all-to-all | bytes 1048576 | tf_op jit(solution)/shard_map/all_to_all | solution.py:97
  203.7 0.7 add_convert_fusion
  (87 shorter events, 3.6 us)
Async XLA Ops:
  6.5 116.1 %copy-start = (bf16[512,512]{1,0:T(8,128)(2,1)S(1)}, bf16[512,512]{1,0:T(8,128)(2,1)}, u32[]{:S(2)}) copy-start(bf16[512,512]{1,0:T(8,128)(2,1)} %param.23) | copy-start | bytes 1572868
  6.6 135.8 %all-gather.7.cloned.1.call-start = ((), (), s32[]{:S(2)}) async-start(), calls=%async_computation.4 | async-start | bytes 11894784 | tf_op jit(solution)/shard_map/all_gather | solution.py:79
  8.5 178.2 %all-gather.9.cloned.1.call-start = ((), (), s32[]{:S(2)}) async-start(), calls=%async_computation.5 | async-start | bytes 5947392 | tf_op jit(solution)/shard_map/all_gather | solution.py:253
  39.2 2.9 %copy-start.1 = (f32[2,2,64,64]{3,2,1,0:T(8,128)}, f32[2,2,64,64]{3,2,1,0:T(8,128)S(1)}, u32[]{:S(2)}) copy-start(f32[2,2,64,64]{3,2,1,0:T(8,128)S(1)} %get-tuple-element.48) | copy-start | bytes 196612
  39.2 92.3 %copy-start.4 = (f32[512]{0:T(512)S(1)}, f32[512]{0:T(512)}, u32[]{:S(2)}) copy-start(f32[512]{0:T(512)} %param.24) | copy-start | bytes 6148
  142.4 8.8 %copy-start.2 = (f32[3,1408]{1,0:T(4,128)S(1)}, f32[3,1408]{1,0:T(4,128)}, u32[]{:S(2)}) copy-start(f32[3,1408]{1,0:T(4,128)} %param.27) | copy-start | bytes 50692
  142.4 8.8 %copy-start.3 = (f32[3,1408]{1,0:T(4,128)S(1)}, f32[3,1408]{1,0:T(4,128)}, u32[]{:S(2)}) copy-start(f32[3,1408]{1,0:T(4,128)} %param.28) | copy-start | bytes 50692
  149.8 2.1 %collective-permute-start = (bf16[2,2816]{1,0:T(2,128)(2,1)S(1)}, bf16[2,2816]{1,0:T(2,128)(2,1)S(1)}, u32[]{:S(2)}, u32[]{:S(2)}) collective-permute-start(bf16[2,2816]{1,0:T(2,128)(2,1)S(1)} %pad_maximum_fusion.1), channel_id=1, source_target_pairs={{0,4},{4,8},{8,12},{12,16},{16,20},{20,24},{24,28},{28,32},{32,36}... | collective-permute-start | bytes 33800 | tf_op jit(solution)/shard_map/ppermute | solution.py:86
Sparse Core Ops, SparseCore 0:
  9.2 106.0 all-gather.6
  117.2 69.4 all-gather.8
where the time goes:
time: 214 us; the launch traced here: 211 us
  blocking collectives  106 us (50%)
  waiting for transfers between devices  36 us (17%)
  local copies, waits for them, and re-layouts  21.3 us (10%)
  other arithmetic  16.6 us (8%)
  matrix products  15.5 us (7%)
  between operations  14 us (7%)
    all_gather x2, blocking collectives, all_in_one(): both, at, found = (lax.all_gather(jnp.concatenate(lines), axis), 0, {})  67.6 us
    all_gather x1, waiting for transfers between devices, on_device(): lax.all_gather(down_weight, SP, axis=1, tiled=True)  34.5 us
    all_to_all x3, blocking collectives, copy_for_each(): return lax.all_to_all(copies, axis, split_axis=0, concat_axis=0, tiled=True)  26.4 us
    all_to_all x1, blocking collectives, summed_on_arrival(): lax.all_to_all(split_up(array, dim, length), axis, 0, 0, tiled=True)  12.2 us
    while x2, local copies, waits for them, and re-layouts  11.2 us
    exp x2, other arithmetic, advance(): jnp.exp(spread)  5.89 us
    dot_general x2, other arithmetic, advance(): jnp.einsum('htk,hsk,htsk->hts', block_queries, block_keys, jnp.exp(spread...  5.7 us
    dot_general x1, matrix products, on_device(): jnp.dot(hidden, lax.all_gather(down_weight, SP, axis=1, tiled=True), pref...  4.73 us
  transfers between devices with their start and end apart: 3, of which 2 were waited for; matrix products, arithmetic and copies ran while one was open for 22% of the time, Pallas kernels for 0%

commit v1 on v0

v1 whole, which is shorter than its diff:
```python
import jax
import jax.numpy as jnp
from jax import lax
from jax.experimental import pallas as pl
from jax.experimental.pallas import tpu as pltpu
from jax.sharding import Mesh
from jax.sharding import PartitionSpec as P

BF = jnp.bfloat16
F32 = jnp.float32
EPS = 1e-06
DK = 64
SP = ("sp_0", "sp_1")
GRP = ("grp_0", "grp_1")
PAIR = ("grp_1", "tp")
HALO = 16
CH = 16


def silu(v):
    return v / (1.0 + jnp.exp(-v))


def nt_dot(a, b):
    return lax.dot_general(a, b, (((1,), (1,)), ((), ())), preferred_element_type=F32)


def tn_dot(a, b):
    return lax.dot_general(a, b, (((0,), (0,)), ((), ())), preferred_element_type=F32)


def dot(a, b):
    return jnp.dot(a, b, preferred_element_type=F32)


def iota(shape, dim):
    return lax.broadcasted_iota(jnp.int32, shape, dim)


def in_order(rows, halo):
    count = rows.shape[0]
    both = jnp.concatenate([rows.astype(F32), halo.astype(F32)], axis=0)
    row = iota(both.shape, 0)
    both = jnp.where((row >= count) & (row < count + HALO - 2), 0.0, both)
    return pltpu.roll(both, 2, 0)


def head_ones(width):
    a = iota((width, width), 0) // DK
    b = iota((width, width), 1) // DK
    return jnp.where(a == b, 1.0, 0.0).astype(BF)


def local_kernel(q_ref, f_ref, v_ref, halo_ref, gap_ref, intra_ref, qd_ref, state_ref):
    count, width = q_ref.shape
    q = silu(in_order(q_ref[...], halo_ref[:, 0:width]))
    f = in_order(f_ref[...], halo_ref[:, width : 2 * width])
    v = in_order(v_ref[...], halo_ref[:, 2 * width : 3 * width])
    rows = q.shape[0]
    k = gap_ref[...] / (1.0 + jnp.exp(f))
    a = 1.0 - k
    la = jnp.log(a)
    row = iota(q.shape, 0)
    lane = iota((CH, width), 1)
    r = la
    step = 1
    while step < rows:
        r = r + jnp.where(row >= step, pltpu.roll(r, step, 0), 0.0)
        step *= 2
    ones = head_ones(width)
    inside = row % CH
    decay = jnp.ones_like(q)
    out = jnp.zeros_like(q)
    for j in range(CH):
        if j:
            decay = decay * (pltpu.roll(a, j - 1, 0) if j > 1 else a)
        kj = pltpu.roll(k, j, 0) if j else k
        vj = pltpu.roll(v, j, 0) if j else v
        term = jnp.where(inside >= j, q * decay * kj, 0.0)
        out = out + dot(term.astype(BF), ones) * vj
    pieces = [out[:CH]]
    vb = v.astype(BF)
    for i in range(1, rows // CH):
        lo = i * CH
        start = r[lo - 1 : lo]
        qi = q[lo : lo + CH] * jnp.exp(r[lo : lo + CH] - start)
        qi = jnp.concatenate([jnp.where(lane < DK, qi, 0.0), jnp.where(lane >= DK, qi, 0.0)], axis=0)
        ki = k[:lo] * jnp.exp(start - r[:lo])
        both = dot(nt_dot(qi.astype(BF), ki.astype(BF)).astype(BF), vb[:lo])
        pieces.append(out[lo : lo + CH] + jnp.where(lane < DK, both[:CH], both[CH:]))
    intra_ref[...] = jnp.concatenate(pieces, axis=0)
    qd_ref[...] = (q * jnp.exp(r)).astype(BF)
    last = r[count - 1 : count]
    kf = (k[:count] * jnp.exp(last - r[:count])).astype(BF)
    full = tn_dot(vb[:count], kf)
    half = iota((DK, width), 1)
    state_ref[:DK] = jnp.where(half < DK, full[:DK], full[DK:]).astype(BF)
    state_ref[DK:] = jnp.broadcast_to(jnp.exp(last), (HALO, width)).astype(BF)


def head_kernel(intra_ref, qd_ref, enter_ref, g_ref, halo_ref, gain_ref, out_ref):
    width = intra_ref.shape[1]
    half = iota((DK, width), 1)
    e = enter_ref[...]
    full = jnp.concatenate([jnp.where(half < DK, e, 0.0), jnp.where(half >= DK, e, 0.0)], axis=0)
    rec = intra_ref[...] + nt_dot(qd_ref[...], full.astype(BF))
    ones = head_ones(width)
    sq = rec * rec
    hi = sq.astype(BF)
    lo = (sq - hi.astype(F32)).astype(BF)
    mean = (dot(hi, ones) + dot(lo, ones)) * (1.0 / DK)
    gate = in_order(g_ref[...], halo_ref[...])
    out = rec * lax.rsqrt(mean + EPS) * gain_ref[...] * silu(gate)
    out_ref[...] = pltpu.roll(out, out.shape[0] - 2, 0).astype(BF)


def stream_kernel(x_ref, *refs):
    n = (len(refs) - 2) // 4
    heads, weights, resid, gains = (refs[i * n : (i + 1) * n] for i in range(4))
    normed_ref, own_ref = refs[4 * n :]
    x = x_ref[0]
    hw = heads[0].shape[1]
    cw = resid[0].shape[1]
    head = jnp.concatenate([h[...] for h in heads], axis=1)
    parts = []
    total = None
    for d in range(n):
        w = jnp.concatenate([weights[d][pl.ds(hw * lax.rem(x + e, n), hw), :] for e in range(n)], axis=0)
        s = resid[d][...].astype(F32) + dot(head, w)
        parts.append(s)
        sq = jnp.sum(s * s, axis=1, keepdims=True)
        total = sq if total is None else total + sq
    own_ref[...] = parts[0][: own_ref.shape[0]]
    scale = lax.rsqrt(total / (n * cw) + EPS)
    for d in range(n):
        g = gains[d][...].astype(F32)
        gain = g[0:1] + g[1:2] + g[2:3]
        normed_ref[:, d * cw : (d + 1) * cw] = (parts[d] * scale * gain).astype(BF)


def mixer_kernel(x_ref, normed_ref, taps_ref, w_hbm, out_ref, w, acc, sems):
    n = out_ref.shape[0]
    groups = out_ref.shape[1]
    count = out_ref.shape[2]
    x = x_ref[0]
    cw = w.shape[0] // n
    up = taps_ref.shape[1]
    half = up // 2
    rows = acc.shape[0] // groups

    def copy(d):
        return pltpu.make_async_copy(
            w_hbm.at[pl.ds(cw * lax.rem(x + d, n), cw), :], w.at[pl.ds(cw * d, cw), :], sems.at[d]
        )

    for d in range(n):
        copy(d).start()
    for d in range(n):
        copy(d).wait()
        part = dot(normed_ref[:, d * cw : (d + 1) * cw], w[d * cw : (d + 1) * cw, :up])
        if d == 0:
            acc[...] = part
        else:
            acc[...] += part
    hidden = []
    for g in range(groups):
        u = acc[g * rows : (g + 1) * rows, :].astype(BF).astype(F32)
        c = (
            taps_ref[0:1] * pltpu.roll(u, 2, 0)
            + taps_ref[1:2] * pltpu.roll(u, 1, 0)
            + taps_ref[2:3] * u
        )[:count]
        gate = pltpu.roll(c, half, 1)[:, :half]
        hidden.append((silu(gate) * c[:, :half]).astype(BF))
    hidden = jnp.concatenate(hidden, axis=0)
    for d in range(n):
        t = nt_dot(hidden, w[d * cw : (d + 1) * cw, up:]).astype(BF)
        for g in range(groups):
            out_ref[d, g] = t[g * count : (g + 1) * count]


def call(kernel, out, *args, scratch=(), specs=None):
    vm = pl.BlockSpec(memory_space=pltpu.VMEM)
    return pl.pallas_call(
        kernel,
        out_shape=out,
        in_specs=specs or [vm] * len(args),
        out_specs=jax.tree.map(lambda _: vm, out),
        scratch_shapes=list(scratch),
    )(*args)


def moved(array, axis, by):
    n = lax.axis_size(axis)
    return lax.ppermute(array, axis, [(i, i + by) for i in range(n) if 0 <= i + by < n])


def from_peers(array):
    n = lax.axis_size("tp")
    return [array] + [
        lax.ppermute(array, "tp", [((i + d) % n, i) for i in range(n)]) for d in range(1, n)
    ]


def from_pair(array):
    return lax.ppermute(array, "grp_1", [(0, 1), (1, 0)])


def own_half(array, dim):
    n = array.shape[dim] // 2
    lo = lax.slice_in_dim(array, 0, n, axis=dim)
    hi = lax.slice_in_dim(array, n, 2 * n, axis=dim)
    return jnp.where(lax.axis_index("grp_1") == 0, lo, hi)


def entering(packed):
    partner = lax.ppermute(packed, "sp_1", [(0, 1), (1, 0)]).astype(F32)
    own = packed.astype(F32)
    second = lax.axis_index("sp_1") == 1

    def parts(p):
        p = p.astype(F32)
        return p[:DK], p[DK : DK + 1]

    first, later = jnp.where(second, partner, own), jnp.where(second, own, partner)
    s0, d0 = parts(first)
    s1, d1 = parts(later)

    def pack(s, d):
        return jnp.concatenate([s, jnp.broadcast_to(d, (HALO, d.shape[1]))], axis=0).astype(BF)

    chip = pack(d1 * s0 + s1, d0 * d1)
    n = lax.axis_size("sp_0")

    def window(p, shifts):
        got = [parts(moved(p, "sp_0", k)) for k in shifts if k < n]
        state, decay = got[-1]
        for s, d in got[-2::-1]:
            state = d * state + s
            decay = d * decay
        return state, decay

    state, decay = window(chip, (1, 2, 3, 4))
    if n > 4:
        before, _ = window(pack(state, decay), (4, 8, 12))
        state = state + decay * before
    return jnp.where(second, d0 * state + s0, state)


def on_device(
    residual_in,
    query_pre,
    forget_pre,
    value_pre,
    gate_pre,
    floor_gap,
    head_gain,
    out_weight,
    norm_gain,
    value_weight,
    gate_weight,
    value_taps,
    gate_taps,
    down_weight,
):
    count, cols = residual_in.shape
    width = query_pre.shape[1]
    rows = count + HALO
    n = lax.axis_size("tp")
    x = lax.axis_index("tp").astype(jnp.int32).reshape(1)
    share = jnp.concatenate(
        [own_half(value_weight, 1), own_half(gate_weight, 1), own_half(down_weight, 0).T], axis=1
    )
    gathered = lax.all_gather(share, SP, axis=0, tiled=True)

    tails = jnp.concatenate(
        [a[count - HALO :] for a in (query_pre, forget_pre, value_pre, gate_pre, residual_in)], axis=1
    )
    halo = moved(tails, SP, 1)
    sd = jax.ShapeDtypeStruct
    intra, qd, packed = call(
        local_kernel,
        (sd((rows, width), F32), sd((rows, width), BF), sd((DK + HALO, width), BF)),
        query_pre,
        forget_pre,
        value_pre,
        halo,
        floor_gap.reshape(1, width),
    )
    enter = entering(packed)
    head = call(
        head_kernel,
        sd((rows, width), BF),
        intra,
        qd,
        enter,
        gate_pre,
        halo[:, 3 * width : 4 * width],
        jnp.tile(head_gain, width // DK).reshape(1, width),
    )
    resid_halo = jnp.where(iota((HALO, cols), 0) < HALO - 2, 0.0, halo[:, 4 * width :].astype(F32))
    resid = jnp.concatenate([residual_in, resid_halo.astype(BF)], axis=0)
    resid = jnp.concatenate([resid, from_pair(resid)], axis=0)
    g0 = lax.reduce_precision(norm_gain, 8, 7)
    g1 = lax.reduce_precision(norm_gain - g0, 8, 7)
    g2 = norm_gain - g0 - g1
    gains = jnp.stack([g0, g1, g2] + [jnp.zeros_like(g0)] * (HALO - 3)).astype(BF)
    weights = from_peers(jnp.concatenate([out_weight, gains], axis=0))
    resids = from_peers(resid)
    heads = from_peers(jnp.concatenate([head, from_pair(head)], axis=0))
    hrows = out_weight.shape[0]
    vm = pl.BlockSpec(memory_space=pltpu.VMEM)
    sm = pl.BlockSpec(memory_space=pltpu.SMEM)
    hbm = pl.BlockSpec(memory_space=pl.ANY)
    normed, own = call(
        stream_kernel,
        (sd((2 * rows, n * cols), BF), sd((count, cols), F32)),
        x,
        *heads,
        *[w[:hrows] for w in weights],
        *resids,
        *[w[hrows:] for w in weights],
        specs=[sm] + [vm] * (4 * n),
    )
    taps = jnp.concatenate([own_half(value_taps, 1), own_half(gate_taps, 1)], axis=1)
    terms = call(
        mixer_kernel,
        sd((n, 2, count, cols), BF),
        x,
        normed,
        taps,
        gathered,
        specs=[sm, vm, vm, hbm],
        scratch=(
            pltpu.VMEM(gathered.shape, BF),
            pltpu.VMEM((2 * rows, taps.shape[1]), F32),
            pltpu.SemaphoreType.DMA((n,)),
        ),
    )
    total = own + terms[0, 0].astype(F32)
    for g in (1, 0):
        for d in range(n):
            if g or d:
                perm = [
                    (p * n + i, (p ^ g) * n + (i + d) % n) for p in range(2) for i in range(n)
                ]
                total = total + lax.ppermute(terms[d, g], PAIR, perm).astype(F32)
    return total.astype(BF)


def solution(mesh):
    groups, seq, tp = (mesh.shape[a] for a in ("grp", "sp", "tp"))
    finer = Mesh(
        mesh.devices.reshape(groups // 2, 2, seq // 2, 2, tp), (*GRP, *SP, "tp")
    )
    rows = P((*GRP, *SP), "tp")
    placed = (
        *[rows] * 5,
        P("tp"),
        P(),
        P(None, "tp"),
        P("tp"),
        P(SP, "tp"),
        P(SP, "tp"),
        P(None, "tp"),
        P(None, "tp"),
        P("tp", SP),
    )
    return jax.shard_map(on_device, mesh=finer, in_specs=placed, out_specs=rows, check_vma=False)
```

time: 214 us -> 154 us (0.72)
  blocking collectives: 106 us -> 0 us
  starting transfers between devices: 1.37 us -> 75.1 us
  waiting for transfers between devices: 36 us -> 18.9 us
  Pallas kernels: 0 us -> 16.7 us
  matrix products: 15.5 us -> 0 us
  other arithmetic: 16.6 us -> 11 us
  local copies, waits for them, and re-layouts: 21.3 us -> 17.3 us
    ppermute x1 -> x27, starting transfers between devices: 1.31 us -> 75.1 us  [the longest x8 49.7 us: moved(): lax.ppermute(array, axis, [(i, i + by) for i in range(n) if 0 <= i + by <...]
    all_gather x2 -> x0, blocking collectives: 67.6 us -> none  [all_in_one(): both, at, found = (lax.all_gather(jnp.concatenate(lines), axis), 0, {})]
    all_to_all x4 -> x0, blocking collectives: 38.5 us -> none  [the longest x3 26.4 us: copy_for_each(): return lax.all_to_all(copies, axis, split_axis=0, concat_axis=0, tiled=True)]
    all_gather x2 -> x1, waiting for transfers between devices: 34.6 us -> 0.02 us  [on_device(): gathered = lax.all_gather(share, SP, axis=0, tiled=True)]
    ppermute x1 -> x27, waiting for transfers between devices: 0.7 us -> 18.9 us  [the longest x7 10 us: on_device(): total = total + lax.ppermute(terms[d, g], PAIR, perm).astype(F32)]
    pallas_call x0 -> x4, Pallas kernels: none -> 16.7 us  [call(): pl.pallas_call(kernel, out_shape=out, in_specs=specs or [vm] * len(args),...]
    dot_general x11 -> x0, matrix products: 15.5 us -> none  [the longest x1 4.73 us: on_device(): jnp.dot(hidden, lax.all_gather(down_weight, SP, axis=1, tiled=True), pref...]
    while x2 -> x0, local copies, waits for them, and re-layouts: 11.2 us -> none
  transfers between devices with their start and end apart: 3 -> 28, of which waited for: 2 -> 14; matrix products, arithmetic and copies ran while one was open for 22% -> 14% of each run, Pallas kernels for 0% -> 6%
where the time goes in v1:
time: 154 us; the launch traced here: 153 us
  starting transfers between devices  75.1 us (49%)
  waiting for transfers between devices  18.9 us (12%)
  local copies, waits for them, and re-layouts  17.3 us (11%)
  Pallas kernels  16.7 us (11%)
  between operations  13.8 us (9%)
  other arithmetic  11 us (7%)
    ppermute x8, starting transfers between devices, moved(): lax.ppermute(array, axis, [(i, i + by) for i in range(n) if 0 <= i + by <...  49.7 us
    pallas_call x4, Pallas kernels, call(): pl.pallas_call(kernel, out_shape=out, in_specs=specs or [vm] * len(args),...  16.7 us
    ppermute x9, starting transfers between devices, from_peers(): lax.ppermute(array, 'tp', [((i + d) % n, i) for i in range(n)])  12.4 us
    ppermute x7, waiting for transfers between devices, on_device(): total = total + lax.ppermute(terms[d, g], PAIR, perm).astype(F32)  10 us
    ppermute x7, starting transfers between devices, on_device(): total = total + lax.ppermute(terms[d, g], PAIR, perm).astype(F32)  7.64 us
    unnamed x22, local copies, waits for them, and re-layouts  4.32 us
    ppermute x2, waiting for transfers between devices, from_pair(): return lax.ppermute(array, 'grp_1', [(0, 1), (1, 0)])  3.57 us
    ppermute x1, starting transfers between devices, entering(): partner = lax.ppermute(packed, 'sp_1', [(0, 1), (1, 0)]).astype(F32)  3.15 us
  transfers between devices with their start and end apart: 28, of which 14 were waited for; matrix products, arithmetic and copies ran while one was open for 14% of the time, Pallas kernels for 6%

profile of v1, /device:TPU:38, one launch (start us, length us, event | category | flops | bytes accessed | tf_op | source)
XLA Modules:
  0.0 152.9 jit_solution(2599534427822524012)
XLA Ops:
  6.6 1.1 select_bitcast_fusion
  7.6 1.2 slice_select_fusion
  8.8 0.8 concatenate.39
  9.7 0.7 constant_dynamic-update-slice_fusion.3
  10.4 0.7 constant_dynamic-update-slice_fusion.2
  11.1 0.7 constant_dynamic-update-slice_fusion.1
  11.8 0.7 constant_dynamic-update-slice_fusion
  12.5 0.7 slice_dynamic-update-slice_fusion
  13.2 1.8 %collective-permute-start = (bf16[16,1024]{1,0:T(8,128)(2,1)S(1)}, bf16[16,1024]{1,0:T(8,128)(2,1)S(1)}, u32[]{:S(2)}, u32[]{:S(2)}) collective-permute-start(bf16[16,1024]{1,0:T(8,128)(2,1)S(1)} %slice_dynamic-update-slice_fusion), channel_id=1, source_target_pairs={{0,4},{4,8},{8,12},{12,16},{16,20},{20,24},{24,28},{28,32},{32,36}... | collective-permute-start | bytes 98312 | tf_op jit(solution)/shard_map/ppermute | solution.py:195
  15.0 0.8 collective-permute-done.halo_ref
  16.5 2.9 %shard_map.136 = (f32[144,128]{1,0:T(8,128)}, bf16[144,128]{1,0:T(8,128)(2,1)}, bf16[80,128]{1,0:T(8,128)(2,1)}) custom-call(bf16[128,128]{1,0:T(8,128)(2,1)} %q_ref.1, bf16[128,128]{1,0:T(8,128)(2,1)} %f_ref.1, bf16[128,128]{1,0:T(8,128)(2,1)} %v_ref.1, bf16[16,1024]{1,0:T(8,128)(2,1)} %copy-done.6, f32[1,128]{1,0:T(1,128)} %bitcast.42), custom_call_target="tpu_custom_call" | custom-call | tf_op jit(solution)/shard_map/pallas_call | solution.py:184
  19.4 3.2 %collective-permute-start.1 = (bf16[80,128]{1,0:T(8,128)(2,1)}, bf16[80,128]{1,0:T(8,128)(2,1)S(1)}, u32[]{:S(2)}, u32[]{:S(2)}) collective-permute-start(bf16[80,128]{1,0:T(8,128)(2,1)} %get-tuple-element.12), channel_id=1, source_target_pairs={{0,4},{4,0},{1,5},{5,1},{2,6},{6,2},{3,7},{7,3},{8,12},{12,8},{9,1... | collective-permute-start | bytes 61448 | tf_op jit(solution)/shard_map/ppermute | solution.py:217
  22.5 0.7 fusion.14
  23.3 2.0 %concatenate.35 = bf16[528,512]{1,0:T(8,128)(2,1)S(1)} concatenate(bf16[512,512]{1,0:T(8,128)(2,1)} %refs_4_.1, bf16[1,512]{1,0:T(2,128)(2,1)S(1)} %stack.22, bf16[1,512]{1,0:T(2,128)(2,1)S(1)} %stack.23, bf16[1,512]{1,0:T(2,128)(2,1)S(1)} %stack.24, bf16[1,512]{1,0:T(2,128)(2,1)S(1)} %stack_broadcast_in_dim.3, bf16[4,512]{1,0:T(4,128)(2,1)S(1)} %stack.25, bf16[8,512]{1,0:T(8,128)(2,1)S(1)} %stack.26), dimensions={0} | concatenate | bytes 1081344 | tf_op jit(solution)/shard_map/concatenate | solution.py:308
  25.2 0.8 collective-permute-start.13
  26.0 0.7 convert_select_fusion.1
  26.8 4.7 %collective-permute-start.2 = (bf16[80,128]{1,0:T(8,128)(2,1)S(1)}, bf16[80,128]{1,0:T(8,128)(2,1)S(1)}, u32[]{:S(2)}, u32[]{:S(2)}) collective-permute-start(bf16[80,128]{1,0:T(8,128)(2,1)S(1)} %pad_maximum_fusion.4), channel_id=1, source_target_pairs={{0,8},{8,16},{16,24},{24,32},{32,40},{40,48},{48,56},{56,64},{64,7... | collective-permute-start | bytes 61448 | tf_op jit(solution)/shard_map/ppermute | solution.py:195
  31.5 8.1 %collective-permute-start.3 = (bf16[80,128]{1,0:T(8,128)(2,1)S(1)}, bf16[80,128]{1,0:T(8,128)(2,1)S(1)}, u32[]{:S(2)}, u32[]{:S(2)}) collective-permute-start(bf16[80,128]{1,0:T(8,128)(2,1)S(1)} %pad_maximum_fusion.4), channel_id=1, source_target_pairs={{0,16},{8,24},{16,32},{24,40},{32,48},{40,56},{48,64},{56,72},{64,... | collective-permute-start | bytes 61448 | tf_op jit(solution)/shard_map/ppermute | solution.py:195
  39.7 9.1 %collective-permute-start.4 = (bf16[80,128]{1,0:T(8,128)(2,1)S(1)}, bf16[80,128]{1,0:T(8,128)(2,1)S(1)}, u32[]{:S(2)}, u32[]{:S(2)}) collective-permute-start(bf16[80,128]{1,0:T(8,128)(2,1)S(1)} %pad_maximum_fusion.4), channel_id=1, source_target_pairs={{0,24},{8,32},{16,40},{24,48},{32,56},{40,64},{48,72},{56,80},{64,... | collective-permute-start | bytes 61448 | tf_op jit(solution)/shard_map/ppermute | solution.py:195
  48.8 10.2 %collective-permute-start.5 = (bf16[80,128]{1,0:T(8,128)(2,1)S(1)}, bf16[80,128]{1,0:T(8,128)(2,1)S(1)}, u32[]{:S(2)}, u32[]{:S(2)}) collective-permute-start(bf16[80,128]{1,0:T(8,128)(2,1)S(1)} %pad_maximum_fusion.4), channel_id=1, source_target_pairs={{0,32},{8,40},{16,48},{24,56},{32,64},{40,72},{48,80},{56,88},{64,... | collective-permute-start | bytes 61448 | tf_op jit(solution)/shard_map/ppermute | solution.py:195
  59.1 0.7 tile.2
  59.7 0.6 reshape_tile.3.gain_ref
  60.3 0.9 collective-permute-start.14
  61.2 2.3 %collective-permute-start.15 = (bf16[528,512]{1,0:T(8,128)(2,1)S(1)}, bf16[528,512]{1,0:T(8,128)(2,1)S(1)}, u32[]{:S(2)}, u32[]{:S(2)}) collective-permute-start(bf16[528,512]{1,0:T(8,128)(2,1)S(1)} %concatenate.35), channel_id=1, source_target_pairs={{3,0},{0,1},{1,2},{2,3},{7,4},{4,5},{5,6},{6,7},{11,8},{8,9},{9,10... | collective-permute-start | bytes 1622024 | tf_op jit(solution)/shard_map/ppermute | solution.py:201
  63.7 7.7 %collective-permute-start.6 = (bf16[80,128]{1,0:T(8,128)(2,1)S(1)}, bf16[80,128]{1,0:T(8,128)(2,1)S(1)}, u32[]{:S(2)}, u32[]{:S(2)}) collective-permute-start(bf16[80,128]{1,0:T(8,128)(2,1)S(1)} %pad_maximum_fusion.5), channel_id=1, source_target_pairs={{0,32},{8,40},{16,48},{24,56},{32,64},{40,72},{48,80},{56,88},{64,... | collective-permute-start | bytes 61448 | tf_op jit(solution)/shard_map/ppermute | solution.py:195
  71.4 6.7 %collective-permute-start.7 = (bf16[80,128]{1,0:T(8,128)(2,1)S(1)}, bf16[80,128]{1,0:T(8,128)(2,1)S(1)}, u32[]{:S(2)}, u32[]{:S(2)}) collective-permute-start(bf16[80,128]{1,0:T(8,128)(2,1)S(1)} %pad_maximum_fusion.5), channel_id=1, source_target_pairs={{0,64},{8,72},{16,80},{24,88},{32,96},{40,104},{48,112},{56,120},{... | collective-permute-start | bytes 61448 | tf_op jit(solution)/shard_map/ppermute | solution.py:195
  78.1 0.8 select_convert_fusion
  78.9 1.3 slice.213.halo_ref
  80.1 1.3 collective-permute-start.8
  81.5 1.5 collective-permute-done.8
  83.0 0.6 add_select_fusion.enter_ref
  83.6 1.9 %shard_map.137 = bf16[144,128]{1,0:T(8,128)(2,1)} custom-call(f32[144,128]{1,0:T(8,128)} %get-tuple-element.10.intra_ref, bf16[144,128]{1,0:T(8,128)(2,1)} %get-tuple-element.11.qd_ref, f32[64,128]{1,0:T(8,128)} %add_select_fusion.enter_ref, bf16[128,128]{1,0:T(8,128)(2,1)} %g_ref.1, bf16[16,128]{1,0:T(8,128)(2,1)} %slice.213.halo_ref, ...), custom_call_target="tpu_custom_call" | custom-call | tf_op jit(solution)/shard_map/pallas_call | solution.py:184
  85.5 2.1 %collective-permute-start.9 = (bf16[144,128]{1,0:T(8,128)(2,1)}, bf16[144,128]{1,0:T(8,128)(2,1)S(1)}, u32[]{:S(2)}, u32[]{:S(2)}) collective-permute-start(bf16[144,128]{1,0:T(8,128)(2,1)} %shard_map.137), channel_id=1, source_target_pairs={{0,128},{128,0},{1,129},{129,1},{2,130},{130,2},{3,131},{131,3},{4... | collective-permute-start | bytes 110600 | tf_op jit(solution)/shard_map/ppermute | solution.py:206
  87.6 0.9 pad_maximum_fusion.1
  88.7 1.5 collective-permute-done.9
  90.1 0.8 pad_maximum_fusion.2.refs_0_
  90.9 0.8 collective-permute-start.10
  91.7 2.1 %collective-permute-done.16 = bf16[144,512]{1,0:T(8,128)(2,1)S(1)} collective-permute-done((bf16[144,512]{1,0:T(8,128)(2,1)S(1)}, bf16[144,512]{1,0:T(8,128)(2,1)S(1)}, u32[]{:S(2)}, u32[]{:S(2)}) %collective-permute-start.16) | collective-permute-done | bytes 147488 | tf_op jit(solution)/shard_map/ppermute | solution.py:206
  93.8 0.9 pad_maximum_fusion.refs_8_
  94.7 1.0 collective-permute-start.17
  95.8 1.3 collective-permute-done.10.refs_1_
  97.1 1.8 %collective-permute-start.18 = (bf16[288,512]{1,0:T(8,128)(2,1)S(1)}, bf16[288,512]{1,0:T(8,128)(2,1)S(1)}, u32[]{:S(2)}, u32[]{:S(2)}) collective-permute-start(bf16[288,512]{1,0:T(8,128)(2,1)S(1)} %pad_maximum_fusion.refs_8_), channel_id=1, source_target_pairs={{2,0},{3,1},{0,2},{1,3},{6,4},{7,5},{4,6},{5,7},{10,8},{11,9},{8,1... | collective-permute-start | bytes 884744 | tf_op jit(solution)/shard_map/ppermute | solution.py:201
  98.9 0.7 collective-permute-start.19
  99.5 0.9 slice_select_fusion.2
  100.4 2.4 %collective-permute-start.11 = (bf16[288,128]{1,0:T(8,128)(2,1)S(1)}, bf16[288,128]{1,0:T(8,128)(2,1)}, u32[]{:S(2)}, u32[]{:S(2)}) collective-permute-start(bf16[288,128]{1,0:T(8,128)(2,1)S(1)} %pad_maximum_fusion.2.refs_0_), channel_id=1, source_target_pairs={{2,0},{3,1},{0,2},{1,3},{6,4},{7,5},{4,6},{5,7},{10,8},{11,9},{8,1... | collective-permute-start | bytes 221192 | tf_op jit(solution)/shard_map/ppermute | solution.py:201
  102.8 1.8 %collective-permute-start.12 = (bf16[288,128]{1,0:T(8,128)(2,1)S(1)}, bf16[288,128]{1,0:T(8,128)(2,1)S(1)}, u32[]{:S(2)}, u32[]{:S(2)}) collective-permute-start(bf16[288,128]{1,0:T(8,128)(2,1)S(1)} %pad_maximum_fusion.2.refs_0_), channel_id=1, source_target_pairs={{3,0},{0,1},{1,2},{2,3},{7,4},{4,5},{5,6},{6,7},{11,8},{8,9},{9,10... | collective-permute-start | bytes 221192 | tf_op jit(solution)/shard_map/ppermute | solution.py:201
  104.6 0.7 pad_maximum_fusion.3.taps_ref
  105.2 1.2 stack.27.refs_12_
  106.5 0.8 slice.214.refs_5_
  107.9 0.8 slice.215.refs_6_
  109.3 0.8 slice.216.refs_7_
  110.8 1.0 collective-permute-done.11.refs_2_
  113.4 4.0 %shard_map.138 = (bf16[288,2048]{1,0:T(8,128)(2,1)}, f32[128,512]{1,0:T(8,128)}) custom-call(s32[1]{0:T(128)} %bitcast.x_ref, bf16[288,128]{1,0:T(8,128)(2,1)} %copy-done.4, bf16[288,128]{1,0:T(8,128)(2,1)} %copy-done.7, bf16[288,128]{1,0:T(8,128)(2,1)} %collective-permute-done.11.refs_2_, bf16[288,128]{1,0:T(8,128)(2,1)} %copy-done.8, ...), custom_call_target="tpu_custom_call" | custom-call | tf_op jit(solution)/shard_map/pallas_call | solution.py:184
  117.5 7.8 %shard_map.139 = bf16[4,2,128,512]{3,2,1,0:T(8,128)(2,1)} custom-call(s32[1]{0:T(128)} %bitcast.x_ref, bf16[288,2048]{1,0:T(8,128)(2,1)} %get-tuple-element.14.normed_ref, f32[3,1408]{1,0:T(4,128)} %pad_maximum_fusion.3.taps_ref, bf16[2048,2112]{1,0:T(8,128)(2,1)} %all-gather.2.cloned.1.call-done.w_hbm), custom_call_target="tpu_custom_call" | custom-call | tf_op jit(solution)/shard_map/pallas_call | solution.py:184
  125.3 1.3 slice_bitcast_fusion.6
  126.9 3.9 %collective-permute-start.25 = (bf16[128,512]{1,0:T(8,128)(2,1)S(1)}, bf16[128,512]{1,0:T(8,128)(2,1)S(1)}, u32[]{:S(2)}, u32[]{:S(2)}) collective-permute-start(bf16[128,512]{1,0:T(8,128)(2,1)S(1)} %get-tuple-element.21), channel_id=1, source_target_pairs={{0,2},{1,3},{2,0},{3,1},{128,130},{129,131},{130,128},{131,129},{4... | collective-permute-start | bytes 393224 | tf_op jit(solution)/shard_map/ppermute | solution.py:347
  130.8 2.2 %collective-permute-start.23 = (bf16[128,512]{1,0:T(8,128)(2,1)S(1)}, bf16[128,512]{1,0:T(8,128)(2,1)S(1)}, u32[]{:S(2)}, u32[]{:S(2)}) collective-permute-start(bf16[128,512]{1,0:T(8,128)(2,1)S(1)} %get-tuple-element.23), channel_id=1, source_target_pairs={{0,131},{1,128},{2,129},{3,130},{128,3},{129,0},{130,1},{131,2},{4... | collective-permute-start | bytes 393224 | tf_op jit(solution)/shard_map/ppermute | solution.py:347
  133.0 0.7 collective-permute-start.22
  133.7 2.4 %collective-permute-done.26 = bf16[128,512]{1,0:T(8,128)(2,1)S(1)} collective-permute-done((bf16[128,512]{1,0:T(8,128)(2,1)S(1)}, bf16[128,512]{1,0:T(8,128)(2,1)S(1)}, u32[]{:S(2)}, u32[]{:S(2)}) %collective-permute-start.26) | collective-permute-done | bytes 131104 | tf_op jit(solution)/shard_map/ppermute | solution.py:347
  136.6 2.7 %collective-permute-done.25 = bf16[128,512]{1,0:T(8,128)(2,1)S(1)} collective-permute-done((bf16[128,512]{1,0:T(8,128)(2,1)S(1)}, bf16[128,512]{1,0:T(8,128)(2,1)S(1)}, u32[]{:S(2)}, u32[]{:S(2)}) %collective-permute-start.25) | collective-permute-done | bytes 131104 | tf_op jit(solution)/shard_map/ppermute | solution.py:347
  139.9 1.1 collective-permute-done.22
  141.0 1.0 collective-permute-done.21
  141.9 2.3 %collective-permute-done.20 = bf16[128,512]{1,0:T(8,128)(2,1)S(1)} collective-permute-done((bf16[128,512]{1,0:T(8,128)(2,1)S(1)}, bf16[128,512]{1,0:T(8,128)(2,1)S(1)}, u32[]{:S(2)}, u32[]{:S(2)}) %collective-permute-start.20) | collective-permute-done | bytes 131104 | tf_op jit(solution)/shard_map/ppermute | solution.py:347
  144.3 1.7 %fusion.7 = bf16[128,512]{1,0:T(8,128)(2,1)} fusion(f32[128,512]{1,0:T(8,128)S(1)} %copy-done.5, bf16[128,512]{1,0:T(8,128)(2,1)S(1)} %collective-permute-done.26, bf16[128,512]{1,0:T(8,128)(2,1)S(1)} %collective-permute-done.25, bf16[128,512]{1,0:T(8,128)(2,1)S(1)} %collective-permute-done.24, bf16[128,512]{1,0:T(8,128)(2,1)S(1)} %collective-permute-done.23, ...), kind=kLoop, calls=%fused_computation.9 | loop fusion | flops 1114112 | bytes 1441792 | tf_op jit(solution)/shard_map/convert_element_type | solution.py:348
  (68 shorter events, 5.8 us)
Async XLA Ops:
  6.5 110.9 %all-gather.2.cloned.1.call-start = ((), (), s32[]{:S(2)}) async-start(), calls=%async_computation | async-start | bytes 9191424 | tf_op jit(solution)/shard_map/all_gather | solution.py:274
  13.2 2.7 %collective-permute-start = (bf16[16,1024]{1,0:T(8,128)(2,1)S(1)}, bf16[16,1024]{1,0:T(8,128)(2,1)S(1)}, u32[]{:S(2)}, u32[]{:S(2)}) collective-permute-start(bf16[16,1024]{1,0:T(8,128)(2,1)S(1)} %slice_dynamic-update-slice_fusion), channel_id=1, source_target_pairs={{0,4},{4,8},{8,12},{12,16},{16,20},{20,24},{24,28},{28,32},{32,36}... | collective-permute-start | bytes 98312 | tf_op jit(solution)/shard_map/ppermute | solution.py:195
  15.9 0.6 copy-start.6
  19.4 6.7 %collective-permute-start.1 = (bf16[80,128]{1,0:T(8,128)(2,1)}, bf16[80,128]{1,0:T(8,128)(2,1)S(1)}, u32[]{:S(2)}, u32[]{:S(2)}) collective-permute-start(bf16[80,128]{1,0:T(8,128)(2,1)} %get-tuple-element.12), channel_id=1, source_target_pairs={{0,4},{4,0},{1,5},{5,1},{2,6},{6,2},{3,7},{7,3},{8,12},{12,8},{9,1... | collective-permute-start | bytes 61448 | tf_op jit(solution)/shard_map/ppermute | solution.py:217
  25.2 73.6 %collective-permute-start.13 = (bf16[528,512]{1,0:T(8,128)(2,1)S(1)}, bf16[528,512]{1,0:T(8,128)(2,1)S(1)}, u32[]{:S(2)}, u32[]{:S(2)}) collective-permute-start(bf16[528,512]{1,0:T(8,128)(2,1)S(1)} %concatenate.35), channel_id=1, source_target_pairs={{1,0},{2,1},{3,2},{0,3},{5,4},{6,5},{7,6},{4,7},{9,8},{10,9},{11,1... | collective-permute-start | bytes 1622024 | tf_op jit(solution)/shard_map/ppermute | solution.py:201
  26.8 33.5 %collective-permute-start.2 = (bf16[80,128]{1,0:T(8,128)(2,1)S(1)}, bf16[80,128]{1,0:T(8,128)(2,1)S(1)}, u32[]{:S(2)}, u32[]{:S(2)}) collective-permute-start(bf16[80,128]{1,0:T(8,128)(2,1)S(1)} %pad_maximum_fusion.4), channel_id=1, source_target_pairs={{0,8},{8,16},{16,24},{24,32},{32,40},{40,48},{48,56},{56,64},{64,7... | collective-permute-start | bytes 61448 | tf_op jit(solution)/shard_map/ppermute | solution.py:195
  31.5 29.7 %collective-permute-start.3 = (bf16[80,128]{1,0:T(8,128)(2,1)S(1)}, bf16[80,128]{1,0:T(8,128)(2,1)S(1)}, u32[]{:S(2)}, u32[]{:S(2)}) collective-permute-start(bf16[80,128]{1,0:T(8,128)(2,1)S(1)} %pad_maximum_fusion.4), channel_id=1, source_target_pairs={{0,16},{8,24},{16,32},{24,40},{32,48},{40,56},{48,64},{56,72},{64,... | collective-permute-start | bytes 61448 | tf_op jit(solution)/shard_map/ppermute | solution.py:195
  39.7 23.9 %collective-permute-start.4 = (bf16[80,128]{1,0:T(8,128)(2,1)S(1)}, bf16[80,128]{1,0:T(8,128)(2,1)S(1)}, u32[]{:S(2)}, u32[]{:S(2)}) collective-permute-start(bf16[80,128]{1,0:T(8,128)(2,1)S(1)} %pad_maximum_fusion.4), channel_id=1, source_target_pairs={{0,24},{8,32},{16,40},{24,48},{32,56},{40,64},{48,72},{56,80},{64,... | collective-permute-start | bytes 61448 | tf_op jit(solution)/shard_map/ppermute | solution.py:195
  48.8 14.7 %collective-permute-start.5 = (bf16[80,128]{1,0:T(8,128)(2,1)S(1)}, bf16[80,128]{1,0:T(8,128)(2,1)S(1)}, u32[]{:S(2)}, u32[]{:S(2)}) collective-permute-start(bf16[80,128]{1,0:T(8,128)(2,1)S(1)} %pad_maximum_fusion.4), channel_id=1, source_target_pairs={{0,32},{8,40},{16,48},{24,56},{32,64},{40,72},{48,80},{56,88},{64,... | collective-permute-start | bytes 61448 | tf_op jit(solution)/shard_map/ppermute | solution.py:195
  60.3 40.0 %collective-permute-start.14 = (bf16[528,512]{1,0:T(8,128)(2,1)S(1)}, bf16[528,512]{1,0:T(8,128)(2,1)S(1)}, u32[]{:S(2)}, u32[]{:S(2)}) collective-permute-start(bf16[528,512]{1,0:T(8,128)(2,1)S(1)} %concatenate.35), channel_id=1, source_target_pairs={{2,0},{3,1},{0,2},{1,3},{6,4},{7,5},{4,6},{5,7},{10,8},{11,9},{8,1... | collective-permute-start | bytes 1622024 | tf_op jit(solution)/shard_map/ppermute | solution.py:201
  61.2 41.6 %collective-permute-start.15 = (bf16[528,512]{1,0:T(8,128)(2,1)S(1)}, bf16[528,512]{1,0:T(8,128)(2,1)S(1)}, u32[]{:S(2)}, u32[]{:S(2)}) collective-permute-start(bf16[528,512]{1,0:T(8,128)(2,1)S(1)} %concatenate.35), channel_id=1, source_target_pairs={{3,0},{0,1},{1,2},{2,3},{7,4},{4,5},{5,6},{6,7},{11,8},{8,9},{9,10... | collective-permute-start | bytes 1622024 | tf_op jit(solution)/shard_map/ppermute | solution.py:201
  63.7 16.5 %collective-permute-start.6 = (bf16[80,128]{1,0:T(8,128)(2,1)S(1)}, bf16[80,128]{1,0:T(8,128)(2,1)S(1)}, u32[]{:S(2)}, u32[]{:S(2)}) collective-permute-start(bf16[80,128]{1,0:T(8,128)(2,1)S(1)} %pad_maximum_fusion.5), channel_id=1, source_target_pairs={{0,32},{8,40},{16,48},{24,56},{32,64},{40,72},{48,80},{56,88},{64,... | collective-permute-start | bytes 61448 | tf_op jit(solution)/shard_map/ppermute | solution.py:195
  71.4 10.0 %collective-permute-start.7 = (bf16[80,128]{1,0:T(8,128)(2,1)S(1)}, bf16[80,128]{1,0:T(8,128)(2,1)S(1)}, u32[]{:S(2)}, u32[]{:S(2)}) collective-permute-start(bf16[80,128]{1,0:T(8,128)(2,1)S(1)} %pad_maximum_fusion.5), channel_id=1, source_target_pairs={{0,64},{8,72},{16,80},{24,88},{32,96},{40,104},{48,112},{56,120},{... | collective-permute-start | bytes 61448 | tf_op jit(solution)/shard_map/ppermute | solution.py:195
  80.1 2.8 %collective-permute-start.8 = (bf16[80,128]{1,0:T(8,128)(2,1)S(1)}, bf16[80,128]{1,0:T(8,128)(2,1)S(1)}, u32[]{:S(2)}, u32[]{:S(2)}) collective-permute-start(bf16[80,128]{1,0:T(8,128)(2,1)S(1)} %pad_maximum_fusion.5), channel_id=1, source_target_pairs={{0,96},{8,104},{16,112},{24,120},{1,97},{9,105},{17,113},{25,121},... | collective-permute-start | bytes 61448 | tf_op jit(solution)/shard_map/ppermute | solution.py:195
  85.5 4.7 %collective-permute-start.9 = (bf16[144,128]{1,0:T(8,128)(2,1)}, bf16[144,128]{1,0:T(8,128)(2,1)S(1)}, u32[]{:S(2)}, u32[]{:S(2)}) collective-permute-start(bf16[144,128]{1,0:T(8,128)(2,1)} %shard_map.137), channel_id=1, source_target_pairs={{0,128},{128,0},{1,129},{129,1},{2,130},{130,2},{3,131},{131,3},{4... | collective-permute-start | bytes 110600 | tf_op jit(solution)/shard_map/ppermute | solution.py:206
  88.5 5.3 %collective-permute-start.16 = (bf16[144,512]{1,0:T(8,128)(2,1)S(1)}, bf16[144,512]{1,0:T(8,128)(2,1)S(1)}, u32[]{:S(2)}, u32[]{:S(2)}) collective-permute-start(bf16[144,512]{1,0:T(8,128)(2,1)S(1)} %pad_maximum_fusion.1), channel_id=1, source_target_pairs={{0,128},{128,0},{1,129},{129,1},{2,130},{130,2},{3,131},{131,3},{4... | collective-permute-start | bytes 442376 | tf_op jit(solution)/shard_map/ppermute | solution.py:206
  90.9 21.5 %copy-start.4 = (bf16[288,128]{1,0:T(8,128)(2,1)}, bf16[288,128]{1,0:T(8,128)(2,1)S(1)}, u32[]{:S(2)}) copy-start(bf16[288,128]{1,0:T(8,128)(2,1)S(1)} %pad_maximum_fusion.2.refs_0_) | copy-start | bytes 221188
  90.9 6.1 %collective-permute-start.10 = (bf16[288,128]{1,0:T(8,128)(2,1)S(1)}, bf16[288,128]{1,0:T(8,128)(2,1)S(1)}, u32[]{:S(2)}, u32[]{:S(2)}) collective-permute-start(bf16[288,128]{1,0:T(8,128)(2,1)S(1)} %pad_maximum_fusion.2.refs_0_), channel_id=1, source_target_pairs={{1,0},{2,1},{3,2},{0,3},{5,4},{6,5},{7,6},{4,7},{9,8},{10,9},{11,1... | collective-permute-start | bytes 221192 | tf_op jit(solution)/shard_map/ppermute | solution.py:201
  94.7 17.7 %copy-start = (bf16[288,512]{1,0:T(8,128)(2,1)}, bf16[288,512]{1,0:T(8,128)(2,1)S(1)}, u32[]{:S(2)}) copy-start(bf16[288,512]{1,0:T(8,128)(2,1)S(1)} %pad_maximum_fusion.refs_8_) | copy-start | bytes 884740
  94.7 17.6 %collective-permute-start.17 = (bf16[288,512]{1,0:T(8,128)(2,1)S(1)}, bf16[288,512]{1,0:T(8,128)(2,1)S(1)}, u32[]{:S(2)}, u32[]{:S(2)}) collective-permute-start(bf16[288,512]{1,0:T(8,128)(2,1)S(1)} %pad_maximum_fusion.refs_8_), channel_id=1, source_target_pairs={{1,0},{2,1},{3,2},{0,3},{5,4},{6,5},{7,6},{4,7},{9,8},{10,9},{11,1... | collective-permute-start | bytes 884744 | tf_op jit(solution)/shard_map/ppermute | solution.py:201
  97.1 15.4 %copy-start.7 = (bf16[288,128]{1,0:T(8,128)(2,1)}, bf16[288,128]{1,0:T(8,128)(2,1)S(1)}, u32[]{:S(2)}) copy-start(bf16[288,128]{1,0:T(8,128)(2,1)S(1)} %collective-permute-done.10.refs_1_) | copy-start | bytes 221188
  97.1 15.3 %collective-permute-start.18 = (bf16[288,512]{1,0:T(8,128)(2,1)S(1)}, bf16[288,512]{1,0:T(8,128)(2,1)S(1)}, u32[]{:S(2)}, u32[]{:S(2)}) collective-permute-start(bf16[288,512]{1,0:T(8,128)(2,1)S(1)} %pad_maximum_fusion.refs_8_), channel_id=1, source_target_pairs={{2,0},{3,1},{0,2},{1,3},{6,4},{7,5},{4,6},{5,7},{10,8},{11,9},{8,1... | collective-permute-start | bytes 884744 | tf_op jit(solution)/shard_map/ppermute | solution.py:201
  98.9 13.5 %collective-permute-start.19 = (bf16[288,512]{1,0:T(8,128)(2,1)S(1)}, bf16[288,512]{1,0:T(8,128)(2,1)S(1)}, u32[]{:S(2)}, u32[]{:S(2)}) collective-permute-start(bf16[288,512]{1,0:T(8,128)(2,1)S(1)} %pad_maximum_fusion.refs_8_), channel_id=1, source_target_pairs={{3,0},{0,1},{1,2},{2,3},{7,4},{4,5},{5,6},{6,7},{11,8},{8,9},{9,10... | collective-permute-start | bytes 884744 | tf_op jit(solution)/shard_map/ppermute | solution.py:201
  100.4 11.4 %collective-permute-start.11 = (bf16[288,128]{1,0:T(8,128)(2,1)S(1)}, bf16[288,128]{1,0:T(8,128)(2,1)}, u32[]{:S(2)}, u32[]{:S(2)}) collective-permute-start(bf16[288,128]{1,0:T(8,128)(2,1)S(1)} %pad_maximum_fusion.2.refs_0_), channel_id=1, source_target_pairs={{2,0},{3,1},{0,2},{1,3},{6,4},{7,5},{4,6},{5,7},{10,8},{11,9},{8,1... | collective-permute-start | bytes 221192 | tf_op jit(solution)/shard_map/ppermute | solution.py:201
  102.8 9.6 %collective-permute-start.12 = (bf16[288,128]{1,0:T(8,128)(2,1)S(1)}, bf16[288,128]{1,0:T(8,128)(2,1)S(1)}, u32[]{:S(2)}, u32[]{:S(2)}) collective-permute-start(bf16[288,128]{1,0:T(8,128)(2,1)S(1)} %pad_maximum_fusion.2.refs_0_), channel_id=1, source_target_pairs={{3,0},{0,1},{1,2},{2,3},{7,4},{4,5},{5,6},{6,7},{11,8},{8,9},{9,10... | collective-permute-start | bytes 221192 | tf_op jit(solution)/shard_map/ppermute | solution.py:201
  112.4 0.6 copy-start.8
  112.4 0.7 copy-start.1
  112.4 0.9 copy-start.2
  112.4 1.0 copy-start.3
  117.4 26.9 %copy-start.5 = (f32[128,512]{1,0:T(8,128)S(1)}, f32[128,512]{1,0:T(8,128)}, u32[]{:S(2)}) copy-start(f32[128,512]{1,0:T(8,128)} %get-tuple-element.13) | copy-start | bytes 786436
  126.6 9.4 %collective-permute-start.26 = (bf16[128,512]{1,0:T(8,128)(2,1)S(1)}, bf16[128,512]{1,0:T(8,128)(2,1)S(1)}, u32[]{:S(2)}, u32[]{:S(2)}) collective-permute-start(bf16[128,512]{1,0:T(8,128)(2,1)S(1)} %get-tuple-element.20), channel_id=1, source_target_pairs={{0,3},{1,0},{2,1},{3,2},{128,131},{129,128},{130,129},{131,130},{4... | collective-permute-start | bytes 393224 | tf_op jit(solution)/shard_map/ppermute | solution.py:347
  126.9 12.4 %collective-permute-start.25 = (bf16[128,512]{1,0:T(8,128)(2,1)S(1)}, bf16[128,512]{1,0:T(8,128)(2,1)S(1)}, u32[]{:S(2)}, u32[]{:S(2)}) collective-permute-start(bf16[128,512]{1,0:T(8,128)(2,1)S(1)} %get-tuple-element.21), channel_id=1, source_target_pairs={{0,2},{1,3},{2,0},{3,1},{128,130},{129,131},{130,128},{131,129},{4... | collective-permute-start | bytes 393224 | tf_op jit(solution)/shard_map/ppermute | solution.py:347
  130.8 8.8 %collective-permute-start.24 = (bf16[128,512]{1,0:T(8,128)(2,1)S(1)}, bf16[128,512]{1,0:T(8,128)(2,1)S(1)}, u32[]{:S(2)}, u32[]{:S(2)}) collective-permute-start(bf16[128,512]{1,0:T(8,128)(2,1)S(1)} %get-tuple-element.22), channel_id=1, source_target_pairs={{0,1},{1,2},{2,3},{3,0},{128,129},{129,130},{130,131},{131,128},{4... | collective-permute-start | bytes 393224 | tf_op jit(solution)/shard_map/ppermute | solution.py:347
  130.8 9.1 %collective-permute-start.23 = (bf16[128,512]{1,0:T(8,128)(2,1)S(1)}, bf16[128,512]{1,0:T(8,128)(2,1)S(1)}, u32[]{:S(2)}, u32[]{:S(2)}) collective-permute-start(bf16[128,512]{1,0:T(8,128)(2,1)S(1)} %get-tuple-element.23), channel_id=1, source_target_pairs={{0,131},{1,128},{2,129},{3,130},{128,3},{129,0},{130,1},{131,2},{4... | collective-permute-start | bytes 393224 | tf_op jit(solution)/shard_map/ppermute | solution.py:347
  133.0 8.0 %collective-permute-start.22 = (bf16[128,512]{1,0:T(8,128)(2,1)S(1)}, bf16[128,512]{1,0:T(8,128)(2,1)S(1)}, u32[]{:S(2)}, u32[]{:S(2)}) collective-permute-start(bf16[128,512]{1,0:T(8,128)(2,1)S(1)} %get-tuple-element.24), channel_id=1, source_target_pairs={{0,130},{1,131},{2,128},{3,129},{128,2},{129,3},{130,0},{131,1},{4... | collective-permute-start | bytes 393224 | tf_op jit(solution)/shard_map/ppermute | solution.py:347
  136.1 5.9 %collective-permute-start.21 = (bf16[128,512]{1,0:T(8,128)(2,1)S(1)}, bf16[128,512]{1,0:T(8,128)(2,1)S(1)}, u32[]{:S(2)}, u32[]{:S(2)}) collective-permute-start(bf16[128,512]{1,0:T(8,128)(2,1)S(1)} %get-tuple-element.25), channel_id=1, source_target_pairs={{0,129},{1,130},{2,131},{3,128},{128,1},{129,2},{130,3},{131,0},{4... | collective-permute-start | bytes 393224 | tf_op jit(solution)/shard_map/ppermute | solution.py:347
  139.3 5.0 %collective-permute-start.20 = (bf16[128,512]{1,0:T(8,128)(2,1)S(1)}, bf16[128,512]{1,0:T(8,128)(2,1)S(1)}, u32[]{:S(2)}, u32[]{:S(2)}) collective-permute-start(bf16[128,512]{1,0:T(8,128)(2,1)S(1)} %get-tuple-element.19), channel_id=1, source_target_pairs={{0,128},{1,129},{2,130},{3,131},{128,0},{129,1},{130,2},{131,3},{4... | collective-permute-start | bytes 393224 | tf_op jit(solution)/shard_map/ppermute | solution.py:347
Sparse Core Ops, SparseCore 0:
  9.8 94.5 all-gather.1
